TPU v7x, 32 devices: a whole 2x2x4 slice. The times are simulated.
32 devices in a mesh: kv: 8 (over z, y), tp: 4 (over x, core).
Axes of the slice: x: 2, y: 2, z: 4, core: 2. Of those that a mesh axis runs over, the one named last changes fastest.
Arguments:
- residual_in: bfloat16 [64, 2048], P(None, ('kv', 'tp')), may hold values from -14 to 14
- delta_state: float32 [64, 32, 128, 128], P('kv', 'tp'), may hold values from -1 to 1
- norm_gain_first: float32 [2048], P('kv'), may hold values from 0.1 to 1.9
- gate_first: bfloat16 [2048, 5632], P('kv', 'tp'), may hold values from -0.125 to 0.125
- up_first: bfloat16 [2048, 5632], P('kv', 'tp'), may hold values from -0.125 to 0.125
- down_first: bfloat16 [5632, 2048], P('tp', 'kv'), may hold values from -0.15625 to 0.15625
- norm_gain_mixer: float32 [2048], P('kv'), may hold values from 0.1 to 1.9
- query_weight: bfloat16 [2048, 2048], P('kv', 'tp'), may hold values from -0.125 to 0.125
- key_weight: bfloat16 [2048, 2048], P('kv', 'tp'), may hold values from -0.125 to 0.125
- value_weight: bfloat16 [2048, 4096], P('kv', 'tp'), may hold values from -0.125 to 0.125
- output_gate_weight: bfloat16 [2048, 4096], P('kv', 'tp'), may hold values from -0.125 to 0.125
- beta_weight: bfloat16 [2048, 32], P('kv'), may hold values from -0.125 to 0.125
- decay_weight: bfloat16 [2048, 32], P('kv'), may hold values from -0.125 to 0.125
- decay_rate: float32 [32], P('tp'), may hold values from -2.3 to 1.1
- decay_bias: float32 [32], P('tp'), may hold values from -1 to 1
- head_gain: float32 [128], replicated, may hold values from 0.1 to 1.9
- out_weight: bfloat16 [4096, 2048], P('tp', 'kv'), may hold values from -0.125 to 0.125
- norm_gain_second: float32 [2048], P('kv'), may hold values from 0.1 to 1.9
- gate_second: bfloat16 [2048, 5632], P('kv', 'tp'), may hold values from -0.125 to 0.125
- up_second: bfloat16 [2048, 5632], P('kv', 'tp'), may hold values from -0.125 to 0.125
- down_second: bfloat16 [5632, 2048], P('tp', 'kv'), may hold values from -0.15625 to 0.15625
Outputs:
- residual_out: bfloat16 [64, 2048], P(None, ('kv', 'tp'))
- delta_state_out: float32 [64, 32, 128, 128], P('kv', 'tp')
All inputs are finite; a program needn't handle non-finite values.
Results may differ from a plain program's by a relative error of at most 0.03.
Values may be sent and summed in bfloat16 or wider, within the bound.
A program may use at most 64 MiB of HBM per device.

v0:
```python
import jax
import jax.numpy as jnp
from jax import lax
from jax.sharding import PartitionSpec as P

D = 2048


epsilon = 1e-06


def activate(summed, square_sums, hidden_cols):
    rowscale = lax.rsqrt(square_sums / D + epsilon)[:, None]
    gate_act = summed[:, :hidden_cols] * rowscale
    up_act = summed[:, hidden_cols:] * rowscale
    return (jax.nn.silu(gate_act) * up_act).astype(jnp.bfloat16)


def feed_forward(residual, norm_gain, gate_weight, up_weight, down_weight, finish):
    as_float = residual.astype(jnp.float32)
    squares = jnp.sum(as_float * as_float, axis=1)
    scaled = (as_float * norm_gain).astype(jnp.bfloat16)
    joined = jnp.concatenate([gate_weight, up_weight], axis=1)
    partial_value = jnp.dot(scaled, joined, preferred_element_type=jnp.float32)
    hidden_cols = gate_weight.shape[1]
    summed, square_sums = (
        lax.psum(partial_value.astype(jnp.bfloat16), "kv").astype(jnp.float32),
        lax.psum(squares.astype(jnp.bfloat16), "kv").astype(jnp.float32),
    )
    hidden = activate(summed, square_sums, hidden_cols)
    projected = jnp.dot(hidden, down_weight, preferred_element_type=jnp.float32).astype(
        jnp.bfloat16
    )
    if finish:
        col_count = residual.shape[1] // lax.axis_size("tp")
        own_cols = lax.dynamic_slice_in_dim(
            as_float, lax.axis_index("tp") * col_count, col_count, 1
        )
        branch = lax.psum_scatter(projected, "tp", scatter_dimension=1, tiled=True).astype(
            jnp.float32
        )
        return (own_cols + 0.5 * branch).astype(jnp.bfloat16)
    branch = lax.psum(projected, "tp").astype(jnp.float32)
    return (as_float + 0.5 * branch).astype(jnp.bfloat16)


def unit_heads(projected, head_size):
    activated = jax.nn.silu(projected).reshape(projected.shape[0], -1, head_size)
    return activated * lax.rsqrt(jnp.sum(activated * activated, axis=-1, keepdims=True) + epsilon)


def delta_step(old_state, key_rows, queries, values, beta_gate, decay_gate):
    faded_state = old_state * decay_gate[:, :, None, None]
    predicted = jnp.einsum("rhab,rha->rhb", faded_state, key_rows, precision=lax.Precision.HIGHEST)
    correction = beta_gate[:, :, None] * (values - predicted)
    updated = faded_state + key_rows[:, :, :, None] * correction[:, :, None, :]
    reading = jnp.einsum("rhab,rha->rhb", updated, queries, precision=lax.Precision.HIGHEST)
    return (updated, reading)


def token_mixer(
    residual,
    norm_gain,
    query_weight,
    key_weight,
    value_weight,
    output_gate_weight,
    beta_weight,
    decay_weight,
    decay_rate,
    decay_bias,
    head_gain,
    out_weight,
    old_state,
):
    as_float = residual.astype(jnp.float32)
    squares = jnp.sum(as_float * as_float, axis=1)
    scaled = (as_float * norm_gain).astype(jnp.bfloat16)
    joined = jnp.concatenate([query_weight, key_weight, value_weight, output_gate_weight], axis=1)
    partial_value = jnp.dot(scaled, joined, preferred_element_type=jnp.float32)
    heads_dev = decay_rate.shape[0]
    head_start = lax.axis_index("tp") * heads_dev
    gate_cols = jnp.concatenate(
        [
            lax.dynamic_slice_in_dim(beta_weight, head_start, heads_dev, 1),
            lax.dynamic_slice_in_dim(decay_weight, head_start, heads_dev, 1),
        ],
        axis=1,
    )
    gate_part = jnp.dot(scaled, gate_cols, preferred_element_type=jnp.float32)
    row_count = old_state.shape[0]
    square_sums = lax.psum(squares, "kv")
    square_sums = lax.dynamic_slice_in_dim(
        square_sums, lax.axis_index("kv") * row_count, row_count, 0
    )
    summed, gate_summed = (
        lax.psum_scatter(
            partial_value.astype(jnp.bfloat16), "kv", scatter_dimension=0, tiled=True
        ).astype(jnp.float32),
        lax.psum_scatter(
            gate_part.astype(jnp.bfloat16), "kv", scatter_dimension=0, tiled=True
        ).astype(jnp.float32),
    )
    rowscale = lax.rsqrt(square_sums / D + epsilon)[:, None]
    summed = summed * rowscale
    gate_summed = gate_summed * rowscale
    head_size = old_state.shape[2]
    key_cols = query_weight.shape[1]
    value_cols = value_weight.shape[1]
    repeat_count = heads_dev // (key_cols // head_size)
    queries = jnp.repeat(
        unit_heads(summed[:, :key_cols], head_size) * head_size ** (-0.5), repeat_count, axis=1
    )
    key_rows = jnp.repeat(
        unit_heads(summed[:, key_cols : 2 * key_cols], head_size), repeat_count, axis=1
    )
    values = jax.nn.silu(summed[:, 2 * key_cols : 2 * key_cols + value_cols]).reshape(
        row_count, heads_dev, head_size
    )
    out_gate = jax.nn.silu(summed[:, 2 * key_cols + value_cols :]).reshape(
        row_count, heads_dev, head_size
    )
    beta_gate = jax.nn.sigmoid(gate_summed[:, :heads_dev])
    decay_gate = jnp.exp(
        -jnp.exp(decay_rate)[None, :]
        * jax.nn.softplus(gate_summed[:, heads_dev:] + decay_bias[None, :])
    )
    new_state, reading = delta_step(old_state, key_rows, queries, values, beta_gate, decay_gate)
    normed = reading * lax.rsqrt(jnp.mean(reading * reading, axis=-1, keepdims=True) + epsilon)
    normed = (
        (normed * head_gain * out_gate)
        .reshape(row_count, heads_dev * head_size)
        .astype(jnp.bfloat16)
    )
    projected = jnp.dot(
        lax.all_gather(normed, "kv", axis=0, tiled=True),
        out_weight,
        preferred_element_type=jnp.float32,
    ).astype(jnp.bfloat16)
    branch = lax.psum(projected, "tp").astype(jnp.float32)
    return ((as_float + branch).astype(jnp.bfloat16), new_state)


def body(
    residual_in,
    delta_state,
    norm_gain_first,
    gate_first,
    up_first,
    down_first,
    norm_gain_mixer,
    query_weight,
    key_weight,
    value_weight,
    output_gate_weight,
    beta_weight,
    decay_weight,
    decay_rate,
    decay_bias,
    head_gain,
    out_weight,
    norm_gain_second,
    gate_second,
    up_second,
    down_second,
):
    columns = lax.all_gather(residual_in, "tp", axis=1, tiled=True)
    after_first = feed_forward(columns, norm_gain_first, gate_first, up_first, down_first, False)
    after_mixer, new_state = token_mixer(
        after_first,
        norm_gain_mixer,
        query_weight,
        key_weight,
        value_weight,
        output_gate_weight,
        beta_weight,
        decay_weight,
        decay_rate,
        decay_bias,
        head_gain,
        out_weight,
        delta_state,
    )
    residual_out = feed_forward(
        after_mixer, norm_gain_second, gate_second, up_second, down_second, True
    )
    return (residual_out, new_state)


def solution(mesh):
    placed = (
        P(None, ("kv", "tp")),
        P("kv", "tp", None, None),
        P("kv"),
        P("kv", "tp"),
        P("kv", "tp"),
        P("tp", "kv"),
        P("kv"),
        P("kv", "tp"),
        P("kv", "tp"),
        P("kv", "tp"),
        P("kv", "tp"),
        P("kv", None),
        P("kv", None),
        P("tp"),
        P("tp"),
        P(),
        P("tp", "kv"),
        P("kv"),
        P("kv", "tp"),
        P("kv", "tp"),
        P("tp", "kv"),
    )
    return jax.shard_map(
        body,
        mesh=mesh,
        in_specs=placed,
        out_specs=(P(None, ("kv", "tp")), P("kv", "tp", None, None)),
        check_vma=False,
    )
```

profile of v0, /device:TPU:0, one launch (start us, length us, event | category | flops | bytes accessed | tf_op | source)
XLA Modules:
  0.0 322.3 jit_solution(16253293188831210375)
XLA Ops:
  7.2 0.9 copy.27
  8.1 6.2 %all_gather.6 = bf16[64,256]{0,1:T(8,128)(2,1)S(1)} all-gather(bf16[64,64]{0,1:T(8,128)(2,1)S(1)} %copy.27), channel_id=1, replica_groups=mesh['kv'=8,'tp'=4] {'tp'}, dimensions={1}, use_global_device_ids=true | all-gather | bytes 40960 | tf_op jit(solution)/shard_map/all_gather | solution.py:167
  14.4 2.6 convolution_convert_fusion.2
  17.2 22.4 %psum.50 = bf16[64]{0:T(256)(128)(2,1)S(1)} all-reduce(bf16[64]{0:T(256)(128)(2,1)S(1)} %fusion.27), channel_id=1, replica_groups=mesh['kv'=8,'tp'=4] {'kv'}, use_global_device_ids=true, to_apply=%region_2.0 | all-reduce | flops 64 | bytes 256 | tf_op jit(solution)/shard_map/psum | solution.py:28
  39.6 1.2 dynamic-slice
  41.5 0.7 constant_dynamic-slice_fusion
  42.2 0.7 exponential_negate_fusion
  42.9 47.6 %all-reduce.4.cloned.1.call-done = bf16[64,2816]{1,0:T(8,128)(2,1)} async-done(((bf16[64,2816]{1,0:T(8,128)(2,1)}), bf16[64,2816]{1,0:T(8,128)(2,1)}) %all-reduce.4.cloned.1.call-update) | async-done | bytes 360464 | tf_op jit(solution)/shard_map/psum | solution.py:27
  90.5 1.0 convert_element_type.96
  91.5 0.3 convolution_convert_fusion.5
  91.9 10.3 %psum.51 = bf16[64,256]{1,0:T(8,128)(2,1)S(1)} all-reduce(bf16[64,256]{1,0:T(8,128)(2,1)S(1)} %convolution_convert_fusion.5), channel_id=1, replica_groups=mesh['kv'=8,'tp'=4] {'tp'}, use_global_device_ids=true, to_apply=%region_3.4 | all-reduce | flops 16384 | bytes 65536 | tf_op jit(solution)/shard_map/psum | solution.py:43
  102.3 1.1 convolution_convert_fusion.1
  103.5 19.7 %psum.52 = f32[64]{0:T(128)S(1)} all-reduce(f32[64]{0:T(128)S(1)} %get-tuple-element.4), channel_id=1, replica_groups=mesh['kv'=8,'tp'=4] {'kv'}, use_global_device_ids=true, to_apply=%region_6.7 | all-reduce | flops 64 | bytes 512 | tf_op jit(solution)/shard_map/psum | solution.py:92
  123.4 33.1 %all-reduce = bf16[64,16]{1,0:T(8,128)(2,1)S(1)} all-reduce(bf16[64,16]{1,0:T(8,128)(2,1)S(1)} %convolution_convert_fusion.6), channel_id=2, replica_groups=mesh['kv'=8,'tp'=4] {'kv'}, use_global_device_ids=true, to_apply=%region_4.5.clone | all-reduce | flops 1024 | bytes 4096
  156.8 8.5 %reduce-scatter.5.cloned.1.call-done = bf16[8,3072]{1,0:T(8,128)(2,1)} async-done(((bf16[64,3072]{1,0:T(8,128)(2,1)}), bf16[8,3072]{1,0:T(8,128)(2,1)}) %reduce-scatter.5.cloned.1.call-update) | async-done | bytes 49168 | tf_op jit(solution)/shard_map/reduce_scatter | solution.py:97
  165.2 1.0 convert_multiply_fusion
  166.5 5.8 %fusion = f32[8,8,1,128]{3,2,1,0:T(1,128)S(1)} fusion(f32[8,8,128,1]{2,3,1,0:T(1,128)S(1)} %bitcast.57, f32[8,8,128,128]{3,2,1,0:T(8,128)} %param.22, f32[8,8]{1,0:T(8,128)S(1)} %get-tuple-element.11), kind=kOutput, calls=%fused_computation.1 | convolution fusion | flops 13631488 | bytes 4260096 | tf_op jit(solution)/shard_map/rhab,rha->rhb/dot_general | solution.py:54
  172.4 1.5 multiply_add_fusion
  174.0 2.0 copy-done.2
  176.0 3.6 %fusion.59 = f32[8,8,1,128]{3,2,1,0:T(1,128)S(1)} fusion(f32[8,8,128,128]{3,2,1,0:T(8,128)S(1)} %multiply_add_fusion, f32[8,8,128,1]{2,3,1,0:T(1,128)S(1)} %bitcast.60), kind=kOutput, calls=%fused_computation.96 | convolution fusion | flops 12582912 | bytes 4259840 | tf_op jit(solution)/shard_map/rhab,rha->rhb/dot_general | solution.py:57
  179.9 30.6 %all_gather.7 = bf16[64,1024]{1,0:T(8,128)(2,1)S(1)} all-gather(bf16[8,1024]{1,0:T(8,128)(2,1)S(1)} %fusion.45), channel_id=1, replica_groups=mesh['kv'=8,'tp'=4] {'kv'}, dimensions={0}, use_global_device_ids=true | all-gather | bytes 147456 | tf_op jit(solution)/shard_map/all_gather | solution.py:136
  210.5 0.2 convolution_convert_fusion.4
  210.8 10.3 %psum.53 = bf16[64,256]{1,0:T(8,128)(2,1)S(1)} all-reduce(bf16[64,256]{1,0:T(8,128)(2,1)S(1)} %convolution_convert_fusion.4), channel_id=1, replica_groups=mesh['kv'=8,'tp'=4] {'tp'}, use_global_device_ids=true, to_apply=%region_11.12 | all-reduce | flops 16384 | bytes 65536 | tf_op jit(solution)/shard_map/psum | solution.py:140
  221.1 1.1 convolution_convert_fusion
  222.4 19.7 %psum.55 = bf16[64]{0:T(256)(128)(2,1)S(1)} all-reduce(bf16[64]{0:T(256)(128)(2,1)S(1)} %get-tuple-element.9), channel_id=1, replica_groups=mesh['kv'=8,'tp'=4] {'kv'}, use_global_device_ids=true, to_apply=%region_14.15 | all-reduce | flops 64 | bytes 256 | tf_op jit(solution)/shard_map/psum | solution.py:28
  242.1 51.1 %all-reduce.6.cloned.1.call-done = bf16[64,2816]{1,0:T(8,128)(2,1)} async-done(((bf16[64,2816]{1,0:T(8,128)(2,1)}), bf16[64,2816]{1,0:T(8,128)(2,1)}) %all-reduce.6.cloned.1.call-update) | async-done | bytes 360464 | tf_op jit(solution)/shard_map/psum | solution.py:27
  293.2 1.0 convert_element_type.117
  294.3 0.3 convolution_convert_fusion.3
  294.6 0.7 copy.37
  295.3 19.0 %reduce-scatter.7.cloned.1.call-done = bf16[64,64]{1,0:T(8,128)(2,1)} async-done(((bf16[256,64]{1,0:T(8,128)(2,1)}), bf16[64,64]{1,0:T(8,128)(2,1)}) %reduce-scatter.7.cloned.1.call-update) | async-done | bytes 8208
  314.3 0.8 copy.38
  315.1 0.7 add_convert_fusion
  (60 shorter events, 1.7 us)
Async XLA Ops:
  7.2 84.4 %copy-start = (bf16[1408,256]{1,0:T(8,128)(2,1)S(1)}, bf16[1408,256]{1,0:T(8,128)(2,1)}, u32[]{:S(2)}) copy-start(bf16[1408,256]{1,0:T(8,128)(2,1)} %param.26) | copy-start | bytes 2162692
  7.2 83.3 %all-reduce.4.cloned.1.call-start = ((), (), s32[]{:S(2)}) async-start(), calls=%async_computation.2 | async-start | bytes 720896 | tf_op jit(solution)/shard_map/psum | solution.py:27
  14.4 87.9 %copy-start.9 = (bf16[256,1024]{1,0:T(8,128)(2,1)S(1)}, bf16[256,1024]{1,0:T(8,128)(2,1)}, u32[]{:S(2)}) copy-start(bf16[256,1024]{1,0:T(8,128)(2,1)} %param.31) | copy-start | bytes 1572868
  14.4 87.9 %copy-start.10 = (bf16[256,1024]{1,0:T(8,128)(2,1)S(1)}, bf16[256,1024]{1,0:T(8,128)(2,1)}, u32[]{:S(2)}) copy-start(bf16[256,1024]{1,0:T(8,128)(2,1)} %param.30) | copy-start | bytes 1572868
  14.4 87.9 %copy-start.11 = (bf16[256,512]{1,0:T(8,128)(2,1)S(1)}, bf16[256,512]{1,0:T(8,128)(2,1)}, u32[]{:S(2)}) copy-start(bf16[256,512]{1,0:T(8,128)(2,1)} %param.29) | copy-start | bytes 786436
  14.4 87.9 %copy-start.12 = (bf16[256,512]{1,0:T(8,128)(2,1)S(1)}, bf16[256,512]{1,0:T(8,128)(2,1)}, u32[]{:S(2)}) copy-start(bf16[256,512]{1,0:T(8,128)(2,1)} %param.28) | copy-start | bytes 786436
  14.4 87.9 %copy-start.13 = (f32[256]{0:T(256)S(1)}, f32[256]{0:T(256)}, u32[]{:S(2)}) copy-start(f32[256]{0:T(256)} %param.27) | copy-start | bytes 3076
  17.0 148.2 %reduce-scatter.5.cloned.1.call-start = ((), (), s32[]{:S(2)}) async-start(), calls=%async_computation.3 | async-start | bytes 442368 | tf_op jit(solution)/shard_map/reduce_scatter | solution.py:97
  91.9 64.7 %copy-start.5 = (f32[8]{0:T(128)S(1)}, f32[8]{0:T(128)}, u32[]{:S(2)}) copy-start(f32[8]{0:T(128)} %param.35) | copy-start | bytes 100
  103.5 189.7 %all-reduce.6.cloned.1.call-start = ((), (), s32[]{:S(2)}) async-start(), calls=%async_computation.4 | async-start | bytes 720896 | tf_op jit(solution)/shard_map/psum | solution.py:27
  165.2 7.2 %copy-start.1 = (f32[8,8,128,128]{3,2,1,0:T(8,128)S(1)}, f32[8,8,128,128]{3,2,1,0:T(8,128)}, u32[]{:S(2)}) copy-start(f32[8,8,128,128]{3,2,1,0:T(8,128)} %param.22) | copy-start | bytes 12582916
  173.9 2.1 copy-start.2
  173.9 5.9 %copy-start.4 = (f32[128]{0:T(128)S(1)}, f32[128]{0:T(128)}, u32[]{:S(2)}) copy-start(f32[128]{0:T(128)} %param.36) | copy-start | bytes 1540
  173.9 36.6 %copy-start.3 = (bf16[1024,256]{1,0:T(8,128)(2,1)S(1)}, bf16[1024,256]{1,0:T(8,128)(2,1)}, u32[]{:S(2)}) copy-start(bf16[1024,256]{1,0:T(8,128)(2,1)} %param.37) | copy-start | bytes 1572868
  173.9 47.1 %copy-start.6 = (bf16[256,1408]{1,0:T(8,128)(2,1)S(1)}, bf16[256,1408]{1,0:T(8,128)(2,1)}, u32[]{:S(2)}) copy-start(bf16[256,1408]{1,0:T(8,128)(2,1)} %param.40) | copy-start | bytes 2162692
  174.0 47.1 %copy-start.7 = (bf16[256,1408]{1,0:T(8,128)(2,1)S(1)}, bf16[256,1408]{1,0:T(8,128)(2,1)}, u32[]{:S(2)}) copy-start(bf16[256,1408]{1,0:T(8,128)(2,1)} %param.39) | copy-start | bytes 2162692
  174.0 47.1 %copy-start.14 = (f32[256]{0:T(256)S(1)}, f32[256]{0:T(256)}, u32[]{:S(2)}) copy-start(f32[256]{0:T(256)} %param.38) | copy-start | bytes 3076
  179.7 114.5 %copy-start.8 = (bf16[1408,256]{1,0:T(8,128)(2,1)S(1)}, bf16[1408,256]{1,0:T(8,128)(2,1)}, u32[]{:S(2)}) copy-start(bf16[1408,256]{1,0:T(8,128)(2,1)} %param.41) | copy-start | bytes 2162692
  222.2 92.1 %reduce-scatter.7.cloned.1.call-start = ((), (), s32[]{:S(2)}) async-start(), calls=%async_computation.5 | async-start | bytes 81920
Sparse Core Ops, SparseCore 0:
  17.1 73.3 all-reduce.3
  103.6 61.5 reduce-scatter.4
  222.3 70.8 all-reduce.5
  295.5 18.7 reduce-scatter.6
where the time goes:
time: 323 us; the launch traced here: 322 us
  blocking collectives  152 us (47%)
  waiting for transfers between devices  126 us (39%)
  matrix products  15.2 us (5%)
  between operations  14.7 us (5%)
  other arithmetic  6.96 us (2%)
  local copies, waits for them, and re-layouts  6.68 us (2%)
    psum x2, waiting for transfers between devices, feed_forward(): lax.psum(partial_value.astype(jnp.bfloat16), 'kv').astype(jnp.float32)  98.7 us
    psum x2, blocking collectives, feed_forward(): lax.psum(squares.astype(jnp.bfloat16), 'kv').astype(jnp.float32)  42.1 us
    unnamed x1, blocking collectives  33.1 us
    all_gather x1, blocking collectives, token_mixer(): lax.all_gather(normed, 'kv', axis=0, tiled=True)  30.6 us
    psum x1, blocking collectives, token_mixer(): square_sums = lax.psum(squares, 'kv')  19.7 us
    unnamed x5, waiting for transfers between devices  19.1 us
    psum x1, blocking collectives, feed_forward(): branch = lax.psum(projected, 'tp').astype(jnp.float32)  10.3 us
    psum x1, blocking collectives, token_mixer(): branch = lax.psum(projected, 'tp').astype(jnp.float32)  10.3 us
  transfers between devices with their start and end apart: 4, of which 4 were waited for; matrix products, arithmetic and copies ran while one was open for 1% of the time, Pallas kernels for 0%

commit v1 on v0

v1 whole, which is shorter than its diff:
```python
import functools

import jax
import jax.numpy as jnp
from jax import lax
from jax.experimental import pallas as pl
from jax.experimental.pallas import tpu as pltpu
from jax.sharding import PartitionSpec as P

EPS = 1e-06
LANES = 128
BF16 = jnp.bfloat16
F32 = jnp.float32


def pad_lanes(size):
    return -(-size // LANES) * LANES


def silu(v):
    return v / (1.0 + jnp.exp(-v))


def dot(a, b):
    return jnp.dot(a, b, preferred_element_type=F32)


def place(rows, cols, shift):
    row = lax.broadcasted_iota(jnp.int32, (rows, cols), 0)
    col = lax.broadcasted_iota(jnp.int32, (rows, cols), 1)
    return jnp.where(col == row + shift, 1.0, 0.0).astype(F32).astype(BF16)


def kernel(
    n_kv,
    n_tp,
    res_ref,
    gain_first_ref,
    gain_mixer_ref,
    gain_second_ref,
    beta_ref,
    decay_ref,
    rate_ref,
    bias_ref,
    head_gain_ref,
    state_hbm,
    gate1_hbm,
    up1_hbm,
    down1_hbm,
    wq_hbm,
    wk_hbm,
    wv_hbm,
    wo_hbm,
    out_hbm,
    gate2_hbm,
    up2_hbm,
    down2_hbm,
    res_out_ref,
    state_out_hbm,
    gate1,
    up1,
    down1,
    wq,
    wk,
    wv,
    wo,
    wout,
    gate2,
    up2,
    down2,
    state,
    res_all,
    s1a,
    r1a,
    s1b,
    r1b,
    hid1,
    par1,
    sma,
    rma,
    smb,
    rmb,
    smc,
    rmc,
    nrm,
    parm,
    s2a,
    r2a,
    s2b,
    r2b,
    hid2,
    par2,
    qk_rows,
    val_rows,
    beta_rows,
    dec_rows,
    read_rows,
    w_sem,
    in_sem,
    out_sem,
    send_sem,
    recv_sem,
):
    kv = lax.axis_index("kv")
    tp = lax.axis_index("tp")
    batch, piece = res_ref.shape
    depth = gate1.shape[0]
    width = depth * n_kv
    own_rows = batch // n_kv
    heads = state.shape[1]
    size = state.shape[2]
    key_cols = wq.shape[1]
    key_heads = key_cols // size
    repeat = heads // key_heads
    val_cols = wv.shape[1]

    weight_pairs = (
        (gate1_hbm, gate1),
        (up1_hbm, up1),
        (down1_hbm, down1),
        (wq_hbm, wq),
        (wk_hbm, wk),
        (wv_hbm, wv),
        (wo_hbm, wo),
        (out_hbm, wout),
        (gate2_hbm, gate2),
        (up2_hbm, up2),
        (down2_hbm, down2),
    )
    loads = [
        pltpu.make_async_copy(src, dst, w_sem.at[i]) for i, (src, dst) in enumerate(weight_pairs)
    ]
    for load in loads[:7]:
        load.start()

    barrier = pltpu.get_barrier_semaphore()
    for off in range(1, n_tp):
        pl.semaphore_signal(
            barrier,
            inc=1,
            device_id={"tp": lax.rem(tp + off, n_tp)},
            device_id_type=pl.DeviceIdType.MESH,
        )
    for off in range(1, n_kv):
        pl.semaphore_signal(
            barrier,
            inc=1,
            device_id={"kv": lax.rem(kv + off, n_kv)},
            device_id_type=pl.DeviceIdType.MESH,
        )
    pl.semaphore_wait(barrier, n_tp - 1 + n_kv - 1)

    pending = []

    def send(event, off, src, dst, axis, peer):
        copy = pltpu.make_async_remote_copy(
            src_ref=src,
            dst_ref=dst,
            send_sem=send_sem.at[event, off],
            recv_sem=recv_sem.at[event, off],
            device_id={axis: peer},
            device_id_type=pl.DeviceIdType.MESH,
        )
        copy.start()
        pending.append(copy)
        return copy

    def gather(event, axis, me, count, own, slots):
        return [
            send(event, off, own, slots.at[me], axis, lax.rem(me + off, count))
            for off in range(1, count)
        ]

    def scatter(event, sends, receives):
        copies = []
        for off in range(1, n_kv):
            peer = lax.rem(kv + off, n_kv)
            copies.append(send(event, off, sends.at[peer], receives.at[kv], "kv", peer))
        return copies

    def collect(copies, sends, receives):
        total = sends[kv].astype(F32)
        for off in range(1, n_kv):
            copies[off - 1].wait_recv()
            source = lax.rem(kv + n_kv - off, n_kv)
            total = total + receives[source].astype(F32)
        return total

    def put(ref, offset, value):
        cols = value.shape[1]
        ref[:, :, offset : offset + cols] = value.reshape(n_kv, own_rows, cols).astype(BF16)

    def square_lanes(residual):
        squares = jnp.sum(residual * residual, axis=1, keepdims=True)
        high = squares.astype(BF16).astype(F32)
        lane = lax.broadcasted_iota(jnp.int32, (batch, LANES), 1)
        return jnp.where(lane == 64, high, jnp.where(lane == 65, squares - high, 0.0))

    def row_scale(extra):
        squares = extra[:, 64:65] + extra[:, 65:66]
        return lax.rsqrt(squares / width + EPS)

    def flat(slots):
        both = slots[...].astype(F32)
        return both.reshape(batch, both.shape[2]).astype(BF16)

    def exchange(event, value, slots):
        slots[tp] = value.astype(BF16)
        copies = gather(event, "tp", tp, n_tp, slots.at[tp], slots)
        for copy in copies:
            copy.wait_recv()
        total = slots[0].astype(F32)
        for other in range(1, n_tp):
            total = total + slots[other].astype(F32)
        return total

    def half_ffn(event, residual, gain_ref, first, w_gate, w_up, w_down, bufs, hid, par):
        send_a, recv_a, send_b, recv_b = bufs
        hidden_cols = w_gate.shape[1]
        up_end = pad_lanes(hidden_cols)
        scaled = (residual * gain_ref[...]).astype(BF16)
        loads[first].wait()
        put(send_a, 0, dot(scaled, w_gate[...]))
        copies_a = scatter(event, send_a, recv_a)
        loads[first + 1].wait()
        put(send_b, 0, dot(scaled, w_up[...]))
        put(send_b, up_end, square_lanes(residual))
        copies_b = scatter(event + 1, send_b, recv_b)
        gate_sum = collect(copies_a, send_a, recv_a)[:, :hidden_cols]
        rest = collect(copies_b, send_b, recv_b)
        scale = row_scale(rest[:, up_end:])
        hidden = (silu(gate_sum * scale) * (rest[:, :hidden_cols] * scale)).astype(BF16)
        hid[kv] = hidden
        copies = gather(event + 2, "kv", kv, n_kv, hid.at[kv], hid)
        loads[first + 2].wait()
        for copy in copies:
            copy.wait_recv()
        branch = exchange(event + 3, dot(flat(hid), w_down[...]), par)
        return (residual + 0.5 * branch).astype(BF16)

    copies = gather(0, "tp", tp, n_tp, res_ref, res_all)
    for load in loads[7:]:
        load.start()
    for row in range(own_rows):
        pltpu.make_async_copy(state_hbm.at[row], state.at[row], in_sem.at[row]).start()
    decay_exp = jnp.exp(rate_ref[...])
    extra_weight = (
        dot(beta_ref[...], place_heads(beta_ref.shape[1], tp * heads, 0, heads))
        + dot(decay_ref[...], place_heads(beta_ref.shape[1], tp * heads, heads, heads))
    ).astype(BF16)
    residual = dot(res_ref[...], place(piece, depth, tp * piece))
    for off in range(1, n_tp):
        copies[off - 1].wait_recv()
        source = lax.rem(tp + n_tp - off, n_tp)
        residual = residual + dot(res_all[source], place(piece, depth, source * piece))

    after_first = half_ffn(
        1, residual, gain_first_ref, 0, gate1, up1, down1, (s1a, r1a, s1b, r1b), hid1, par1
    ).astype(F32)

    scaled = (after_first * gain_mixer_ref[...]).astype(BF16)
    loads[3].wait()
    put(sma, 0, dot(scaled, wq[...]))
    loads[4].wait()
    put(sma, key_cols, dot(scaled, wk[...]))
    put(sma, 2 * key_cols, dot(scaled, extra_weight) + square_lanes(after_first))
    copies_a = scatter(5, sma, rma)
    loads[5].wait()
    put(smb, 0, dot(scaled, wv[...]))
    copies_b = scatter(6, smb, rmb)
    loads[6].wait()
    put(smc, 0, dot(scaled, wo[...]))
    copies_c = scatter(7, smc, rmc)

    keys_sum = collect(copies_a, sma, rma)
    extra = keys_sum[:, 2 * key_cols :]
    scale = row_scale(extra)
    for head in range(key_heads):
        for slot, start, factor in (
            (head, head * size, size ** (-0.5)),
            (key_heads + head, key_cols + head * size, 1.0),
        ):
            act = silu(keys_sum[:, start : start + size] * scale)
            unit = act * lax.rsqrt(jnp.sum(act * act, axis=1, keepdims=True) + EPS)
            qk_rows[:, slot, :] = unit * factor
    gates = extra * scale
    beta_pre = gates[:, :heads]
    decay_pre = gates[:, heads : 2 * heads] + bias_ref[...]
    beta_gate = 1.0 / (1.0 + jnp.exp(-beta_pre))
    softplus = jnp.maximum(decay_pre, 0.0) + jnp.log1p(jnp.exp(-jnp.abs(decay_pre)))
    decay_gate = jnp.exp(-decay_exp * softplus)
    for head in range(heads):
        beta_rows[:, head, :] = jnp.broadcast_to(beta_gate[:, head : head + 1], (own_rows, size))
        dec_rows[:, head, :] = jnp.broadcast_to(decay_gate[:, head : head + 1], (own_rows, size))
    values = silu(collect(copies_b, smb, rmb) * scale)
    for head in range(heads):
        val_rows[:, head, :] = values[:, head * size : (head + 1) * size]

    def step(row, carry):
        pltpu.make_async_copy(state_hbm.at[row], state.at[row], in_sem.at[row]).wait()
        columns = qk_rows[row].T
        row_vals, row_beta, row_dec = val_rows[row], beta_rows[row], dec_rows[row]
        for head in range(heads):
            kh = head // repeat
            key_col = columns[:, key_heads + kh : key_heads + kh + 1]
            query_col = columns[:, kh : kh + 1]
            faded = state[row, head] * row_dec[head : head + 1, :]
            predicted = jnp.sum(faded * key_col, axis=0, keepdims=True)
            correction = row_beta[head : head + 1, :] * (row_vals[head : head + 1, :] - predicted)
            updated = faded + key_col * correction
            state[row, head] = updated
            read_rows[row, head : head + 1, :] = jnp.sum(updated * query_col, axis=0, keepdims=True)
        pltpu.make_async_copy(state.at[row], state_out_hbm.at[row], out_sem.at[row]).start()
        return carry

    lax.fori_loop(0, own_rows, step, 0)

    out_gate = silu(collect(copies_c, smc, rmc) * scale)
    for head in range(heads):
        reading = read_rows[:, head, :]
        mean = jnp.mean(reading * reading, axis=1, keepdims=True)
        normed = reading * lax.rsqrt(mean + EPS) * head_gain_ref[...]
        cols = slice(head * size, (head + 1) * size)
        nrm[kv, :, cols] = (normed * out_gate[:, cols]).astype(BF16)
    copies = gather(8, "kv", kv, n_kv, nrm.at[kv], nrm)
    loads[7].wait()
    for copy in copies:
        copy.wait_recv()
    branch = exchange(9, dot(flat(nrm), wout[...]), parm)
    after_mixer = (after_first + branch).astype(BF16).astype(F32)

    final = half_ffn(
        10, after_mixer, gain_second_ref, 8, gate2, up2, down2, (s2a, r2a, s2b, r2b), hid2, par2
    )
    row_id = lax.broadcasted_iota(jnp.int32, (depth, piece), 0)
    col_id = lax.broadcasted_iota(jnp.int32, (depth, piece), 1)
    pick = jnp.where(row_id == col_id + tp * piece, 1.0, 0.0).astype(F32).astype(BF16)
    res_out_ref[...] = dot(final, pick).astype(BF16)

    for copy in pending:
        copy.wait_send()

    def drain(row, carry):
        pltpu.make_async_copy(state.at[row], state_out_hbm.at[row], out_sem.at[row]).wait()
        return carry

    lax.fori_loop(0, own_rows, drain, 0)


def place_heads(rows, first, lane_start, count):
    row = lax.broadcasted_iota(jnp.int32, (rows, LANES), 0)
    col = lax.broadcasted_iota(jnp.int32, (rows, LANES), 1)
    inside = (col >= lane_start) & (col < lane_start + count)
    hit = inside & (row == col - lane_start + first)
    return jnp.where(hit, 1.0, 0.0).astype(F32).astype(BF16)


def body(
    n_kv,
    n_tp,
    residual_in,
    delta_state,
    norm_gain_first,
    gate_first,
    up_first,
    down_first,
    norm_gain_mixer,
    query_weight,
    key_weight,
    value_weight,
    output_gate_weight,
    beta_weight,
    decay_weight,
    decay_rate,
    decay_bias,
    head_gain,
    out_weight,
    norm_gain_second,
    gate_second,
    up_second,
    down_second,
):
    batch, piece = residual_in.shape
    depth, hidden = gate_first.shape
    own_rows, heads, size, _ = delta_state.shape
    key_cols = query_weight.shape[1]
    val_cols = value_weight.shape[1]
    key_heads = key_cols // size
    hp = pad_lanes(hidden)

    def like(x):
        return pltpu.VMEM(x.shape, x.dtype)

    def slots(cols):
        return pltpu.VMEM((n_kv, own_rows, cols), BF16)

    def row_buf(count):
        return pltpu.VMEM((own_rows, count, size), F32)

    tp_slots = pltpu.VMEM((n_tp, batch, depth), BF16)
    ffn_bufs = [slots(hp)] * 2 + [slots(hp + LANES)] * 2 + [slots(hidden), tp_slots]
    mixer_bufs = (
        [slots(2 * key_cols + LANES)] * 2
        + [slots(val_cols)] * 4
        + [slots(heads * size), tp_slots]
    )
    big = (
        gate_first,
        up_first,
        down_first,
        query_weight,
        key_weight,
        value_weight,
        output_gate_weight,
        out_weight,
        gate_second,
        up_second,
        down_second,
    )
    small = (
        residual_in,
        norm_gain_first[None, :],
        norm_gain_mixer[None, :],
        norm_gain_second[None, :],
        beta_weight,
        decay_weight,
        decay_rate[None, :],
        decay_bias[None, :],
        head_gain[None, :],
    )
    vmem = pl.BlockSpec(memory_space=pltpu.VMEM)
    hbm = pl.BlockSpec(memory_space=pl.ANY)
    most = max(n_kv, n_tp)
    return pl.pallas_call(
        functools.partial(kernel, n_kv, n_tp),
        out_shape=(
            jax.ShapeDtypeStruct(residual_in.shape, BF16),
            jax.ShapeDtypeStruct(delta_state.shape, F32),
        ),
        in_specs=[vmem] * len(small) + [hbm] * (1 + len(big)),
        out_specs=(vmem, hbm),
        scratch_shapes=[like(x) for x in big]
        + [like(delta_state), pltpu.VMEM((n_tp, batch, piece), BF16)]
        + ffn_bufs
        + mixer_bufs
        + ffn_bufs
        + [row_buf(2 * key_heads), row_buf(heads), row_buf(heads), row_buf(heads), row_buf(heads)]
        + [
            pltpu.SemaphoreType.DMA((len(big),)),
            pltpu.SemaphoreType.DMA((own_rows,)),
            pltpu.SemaphoreType.DMA((own_rows,)),
            pltpu.SemaphoreType.DMA((14, most)),
            pltpu.SemaphoreType.DMA((14, most)),
        ],
        compiler_params=pltpu.CompilerParams(
            collective_id=0, has_side_effects=True, vmem_limit_bytes=60 * 1024 * 1024
        ),
        name="layer",
    )(*small, delta_state, *big)


def solution(mesh):
    placed = (
        P(None, ("kv", "tp")),
        P("kv", "tp", None, None),
        P("kv"),
        P("kv", "tp"),
        P("kv", "tp"),
        P("tp", "kv"),
        P("kv"),
        P("kv", "tp"),
        P("kv", "tp"),
        P("kv", "tp"),
        P("kv", "tp"),
        P("kv", None),
        P("kv", None),
        P("tp"),
        P("tp"),
        P(),
        P("tp", "kv"),
        P("kv"),
        P("kv", "tp"),
        P("kv", "tp"),
        P("tp", "kv"),
    )
    return jax.shard_map(
        functools.partial(body, mesh.shape["kv"], mesh.shape["tp"]),
        mesh=mesh,
        in_specs=placed,
        out_specs=(P(None, ("kv", "tp")), P("kv", "tp", None, None)),
        check_vma=False,
    )
```

time: 323 us -> 82.4 us (0.26)
  blocking collectives: 152 us -> 0 us
  waiting for transfers between devices: 126 us -> 0 us
  Pallas kernels: 0 us -> 72.4 us
  matrix products: 15.2 us -> 0 us
  between operations: 14.7 us -> 0.64 us
  other arithmetic: 6.96 us -> 0 us
    psum x2 -> x0, waiting for transfers between devices: 98.7 us -> none  [feed_forward(): lax.psum(partial_value.astype(jnp.bfloat16), 'kv').astype(jnp.float32)]
    psum x5 -> x0, blocking collectives: 82.4 us -> none  [the longest x2 42.1 us: feed_forward(): lax.psum(squares.astype(jnp.bfloat16), 'kv').astype(jnp.float32)]
    pallas_call x0 -> x1, Pallas kernels: none -> 72.4 us  [body(): pl.pallas_call(functools.partial(kernel, n_kv, n_tp), out_shape=(jax.Shap...]
    all_gather x2 -> x0, blocking collectives: 36.8 us -> none  [the longest x1 30.6 us: token_mixer(): lax.all_gather(normed, 'kv', axis=0, tiled=True)]
    unnamed x1 -> x0, blocking collectives: 33.1 us -> none
    unnamed x5 -> x0, waiting for transfers between devices: 19.1 us -> none
    dot_general x9 -> x0, matrix products: 15.2 us -> none  [the longest x1 5.81 us: delta_step(): jnp.einsum('rhab,rha->rhb', faded_state, key_rows, precision=lax.Precisio...]
    reduce_scatter x1 -> x0, waiting for transfers between devices: 8.47 us -> none  [token_mixer(): lax.psum_scatter(partial_value.astype(jnp.bfloat16), 'kv', scatter_dimens...]
  transfers between devices with their start and end apart: 4 -> 0, of which waited for: 4 -> 0; matrix products, arithmetic and copies ran while one was open for 1% -> 0% of each run, Pallas kernels for 0% -> 0%
where the time goes in v1:
time: 82.4 us; the launch traced here: 82 us
  Pallas kernels  72.4 us (88%)
  local copies, waits for them, and re-layouts  8.93 us (11%)
    pallas_call x1, Pallas kernels, body(): pl.pallas_call(functools.partial(kernel, n_kv, n_tp), out_shape=(jax.Shap...  72.4 us
    unnamed x4, local copies, waits for them, and re-layouts  8.93 us

profile of v1, /device:TPU:0, one launch (start us, length us, event | category | flops | bytes accessed | tf_op | source)
XLA Modules:
  0.0 82.0 jit_solution(1555396890053972793)
XLA Ops:
  0.6 1.5 %copy.23.beta_ref = bf16[256,32]{1,0:T(8,128)(2,1)} copy(bf16[256,32]{0,1:T(8,128)(2,1)} %param.32) | data formatting | bytes 32768 | tf_op args[11]
  2.1 1.5 %copy.24.decay_ref = bf16[256,32]{1,0:T(8,128)(2,1)} copy(bf16[256,32]{0,1:T(8,128)(2,1)} %param.33) | data formatting | bytes 32768 | tf_op args[12]
  3.5 72.4 %layer.1 = (bf16[64,64]{1,0:T(8,128)(2,1)}, f32[8,8,128,128]{3,2,1,0:T(8,128)}) custom-call(bf16[64,64]{1,0:T(8,128)(2,1)} %res_ref.1, f32[1,256]{1,0:T(1,128)} %bitcast.6, f32[1,256]{1,0:T(1,128)} %bitcast.7, f32[1,256]{1,0:T(1,128)} %bitcast.8, bf16[256,32]{1,0:T(8,128)(2,1)} %copy.23.beta_ref, bf16[256,32]{1,0:T(8,128)(2,1)} %copy.24.decay_ref, ...), custom_call_target="tpu_custom_call" | custom-call | tf_op jit(solution)/shard_map/layer/pallas_call | solution.py:434
  75.9 1.3 %copy.27 = bf16[64,64]{1,0:T(8,128)(2,1)} copy(bf16[64,64]{1,0:T(8,128)(2,1)} %get-tuple-element.4) | data formatting | bytes 16384
  77.3 4.7 %copy.28 = f32[8,8,128,128]{3,2,1,0:T(8,128)} copy(f32[8,8,128,128]{3,2,1,0:T(8,128)} %get-tuple-element.5) | data formatting | bytes 8388608

commit v2 on v1

--- a/solution.py
+++ b/solution.py
@@ -23,6 +23,23 @@
 
 def dot(a, b):
     return jnp.dot(a, b, preferred_element_type=F32)
+
+
+def dot_first(a, b):
+    return lax.dot_general(a, b, (((0,), (0,)), ((), ())), preferred_element_type=F32)
+
+
+def inner_size(count):
+    size = 1
+    while size * size * 4 <= count and count % (size * 2) == 0:
+        size *= 2
+    return size
+
+
+def ffn_chunks(cols):
+    units = -(-cols // LANES)
+    cut = -(-units // 2) * LANES
+    return ((0, cut), (cut, cols - cut)) if cut < cols else ((0, cols),)
 
 
 def place(rows, cols, shift):
@@ -70,39 +87,37 @@
     down2,
     state,
     res_all,
-    s1a,
-    r1a,
-    s1b,
-    r1b,
-    hid1,
-    par1,
-    sma,
-    rma,
-    smb,
-    rmb,
-    smc,
-    rmc,
-    nrm,
-    parm,
-    s2a,
-    r2a,
-    s2b,
-    r2b,
-    hid2,
-    par2,
-    qk_rows,
-    val_rows,
-    beta_rows,
-    dec_rows,
-    read_rows,
-    w_sem,
-    in_sem,
-    out_sem,
-    send_sem,
-    recv_sem,
+    *rest,
 ):
+    n_in = inner_size(n_kv)
+    n_out = n_kv // n_in
+    chunks = len(ffn_chunks(gate1.shape[1]))
+    rest = list(rest)
+
+    def take(count):
+        taken = rest[:count]
+        del rest[:count]
+        return taken
+
+    ffn1 = take(5 * chunks)
+    ffn2 = take(5 * chunks)
+    mixer = take(12)
+    par1, parm, fin_send, fin_recv, nrm = take(5)
+    (
+        qk_rows,
+        val_rows,
+        beta_rows,
+        dec_rows,
+        read_rows,
+        w_sem,
+        in_sem,
+        out_sem,
+        send_sem,
+        recv_sem,
+    ) = rest
     kv = lax.axis_index("kv")
     tp = lax.axis_index("tp")
+    outer, inner = kv // n_in, lax.rem(kv, n_in)
     batch, piece = res_ref.shape
     depth = gate1.shape[0]
     width = depth * n_kv
@@ -171,24 +186,63 @@
             for off in range(1, count)
         ]
 
-    def scatter(event, sends, receives):
-        copies = []
-        for off in range(1, n_kv):
-            peer = lax.rem(kv + off, n_kv)
-            copies.append(send(event, off, sends.at[peer], receives.at[kv], "kv", peer))
-        return copies
-
-    def collect(copies, sends, receives):
-        total = sends[kv].astype(F32)
-        for off in range(1, n_kv):
-            copies[off - 1].wait_recv()
-            source = lax.rem(kv + n_kv - off, n_kv)
-            total = total + receives[source].astype(F32)
-        return total
-
     def put(ref, offset, value):
         cols = value.shape[1]
-        ref[:, :, offset : offset + cols] = value.reshape(n_kv, own_rows, cols).astype(BF16)
+        parts = value.reshape(n_out, n_in, own_rows, cols).astype(BF16)
+        for side in range(n_in):
+            ref[side, :, :, offset : offset + cols] = parts[:, side]
+
+    def scatter_inner(event, bufs):
+        copies = []
+        for off in range(1, n_in):
+            side = lax.rem(inner + off, n_in)
+            peer = outer * n_in + side
+            copies.append(send(event, off, bufs[0].at[side], bufs[1].at[inner], "kv", peer))
+        return copies
+
+    def scatter_outer(event, copies, bufs):
+        mine, theirs, send_buf, recv_buf = bufs[:4]
+        total = mine[inner].astype(F32)
+        for off in range(1, n_in):
+            copies[off - 1].wait_recv()
+            total = total + theirs[lax.rem(inner + n_in - off, n_in)].astype(F32)
+        send_buf[...] = total.astype(BF16)
+        sent = []
+        for off in range(1, n_out):
+            line = lax.rem(outer + off, n_out)
+            peer = line * n_in + inner
+            sent.append(send(event, off, send_buf.at[line], recv_buf.at[outer], "kv", peer))
+        return sent
+
+    def collect(copies, bufs):
+        send_buf, recv_buf = bufs[2:4]
+        total = send_buf[outer].astype(F32)
+        for off in range(1, n_out):
+            copies[off - 1].wait_recv()
+            total = total + recv_buf[lax.rem(outer + n_out - off, n_out)].astype(F32)
+        return total
+
+    def spread(event, slots):
+        line = []
+        for off in range(1, n_out):
+            peer = lax.rem(outer + off, n_out) * n_in + inner
+            line.append(send(event, off, slots.at[kv], slots.at[kv], "kv", peer))
+        near = []
+        for off in range(1, n_in):
+            peer = outer * n_in + lax.rem(inner + off, n_in)
+            near.append(send(event + 1, off, slots.at[kv], slots.at[kv], "kv", peer))
+        return line, near
+
+    def relay(event, line, slots):
+        passed = []
+        for off in range(1, n_out):
+            line[off - 1].wait_recv()
+            slot = lax.rem(outer + n_out - off, n_out) * n_in + inner
+            for side in range(1, n_in):
+                peer = outer * n_in + lax.rem(inner + side, n_in)
+                index = (off - 1) * (n_in - 1) + side - 1
+                passed.append(send(event, index, slots.at[slot], slots.at[slot], "kv", peer))
+        return passed
 
     def square_lanes(residual):
         squares = jnp.sum(residual * residual, axis=1, keepdims=True)
@@ -214,29 +268,50 @@
             total = total + slots[other].astype(F32)
         return total
 
-    def half_ffn(event, residual, gain_ref, first, w_gate, w_up, w_down, bufs, hid, par):
-        send_a, recv_a, send_b, recv_b = bufs
-        hidden_cols = w_gate.shape[1]
-        up_end = pad_lanes(hidden_cols)
+    def pick(peer):
+        row = lax.broadcasted_iota(jnp.int32, (depth, piece), 0)
+        col = lax.broadcasted_iota(jnp.int32, (depth, piece), 1)
+        return jnp.where(row == col + peer * piece, 1.0, 0.0).astype(F32).astype(BF16)
+
+    def half_ffn(event, residual, gain_ref, first, w_gate, w_up, w_down, bufs):
+        spans = ffn_chunks(w_gate.shape[1])
         scaled = (residual * gain_ref[...]).astype(BF16)
-        loads[first].wait()
-        put(send_a, 0, dot(scaled, w_gate[...]))
-        copies_a = scatter(event, send_a, recv_a)
-        loads[first + 1].wait()
-        put(send_b, 0, dot(scaled, w_up[...]))
-        put(send_b, up_end, square_lanes(residual))
-        copies_b = scatter(event + 1, send_b, recv_b)
-        gate_sum = collect(copies_a, send_a, recv_a)[:, :hidden_cols]
-        rest = collect(copies_b, send_b, recv_b)
-        scale = row_scale(rest[:, up_end:])
-        hidden = (silu(gate_sum * scale) * (rest[:, :hidden_cols] * scale)).astype(BF16)
-        hid[kv] = hidden
-        copies = gather(event + 2, "kv", kv, n_kv, hid.at[kv], hid)
+        near, line, going = [], [], []
+        for i, (start, cols) in enumerate(spans):
+            own = bufs[5 * i : 5 * i + 5]
+            step = pad_lanes(cols)
+            if i == 0:
+                loads[first].wait()
+            put(own[0], 0, dot(scaled, w_gate[:, start : start + cols]))
+            if i == 0:
+                loads[first + 1].wait()
+            put(own[0], step, dot(scaled, w_up[:, start : start + cols]))
+            if i == 0:
+                put(own[0], 2 * step, square_lanes(residual))
+            near.append(scatter_inner(event + 5 * i, own))
+        for i in range(len(spans)):
+            line.append(scatter_outer(event + 5 * i + 1, near[i], bufs[5 * i : 5 * i + 5]))
+        scale = None
+        for i, (start, cols) in enumerate(spans):
+            own = bufs[5 * i : 5 * i + 5]
+            step = pad_lanes(cols)
+            total = collect(line[i], own)
+            if i == 0:
+                scale = row_scale(total[:, 2 * step :])
+            gate_act = total[:, :cols] * scale
+            own[4][kv] = (silu(gate_act) * (total[:, step : step + cols] * scale)).astype(BF16)
+            going.append(spread(event + 5 * i + 2, own[4]))
+        passed = [
+            relay(event + 5 * i + 4, going[i][0], bufs[5 * i + 4]) for i in range(len(spans))
+        ]
         loads[first + 2].wait()
-        for copy in copies:
-            copy.wait_recv()
-        branch = exchange(event + 3, dot(flat(hid), w_down[...]), par)
-        return (residual + 0.5 * branch).astype(BF16)
+        product = None
+        for i, (start, cols) in enumerate(spans):
+            for copy in going[i][1] + passed[i]:
+                copy.wait_recv()
+            part = dot(flat(bufs[5 * i + 4]), w_down[start : start + cols, :])
+            product = part if product is None else product + part
+        return product
 
     copies = gather(0, "tp", tp, n_tp, res_ref, res_all)
     for load in loads[7:]:
@@ -245,8 +320,8 @@
         pltpu.make_async_copy(state_hbm.at[row], state.at[row], in_sem.at[row]).start()
     decay_exp = jnp.exp(rate_ref[...])
     extra_weight = (
-        dot(beta_ref[...], place_heads(beta_ref.shape[1], tp * heads, 0, heads))
-        + dot(decay_ref[...], place_heads(beta_ref.shape[1], tp * heads, heads, heads))
+        dot_first(beta_ref[...], place_heads(beta_ref.shape[0], tp * heads, 0, heads))
+        + dot_first(decay_ref[...], place_heads(beta_ref.shape[0], tp * heads, heads, heads))
     ).astype(BF16)
     residual = dot(res_ref[...], place(piece, depth, tp * piece))
     for off in range(1, n_tp):
@@ -254,25 +329,30 @@
         source = lax.rem(tp + n_tp - off, n_tp)
         residual = residual + dot(res_all[source], place(piece, depth, source * piece))
 
-    after_first = half_ffn(
-        1, residual, gain_first_ref, 0, gate1, up1, down1, (s1a, r1a, s1b, r1b), hid1, par1
-    ).astype(F32)
+    product = half_ffn(1, residual, gain_first_ref, 0, gate1, up1, down1, ffn1)
+    e = 1 + 5 * chunks
+    branch = exchange(e, product, par1)
+    after_first = (residual + 0.5 * branch).astype(BF16).astype(F32)
 
     scaled = (after_first * gain_mixer_ref[...]).astype(BF16)
+    bufs_a, bufs_b, bufs_c = mixer[:4], mixer[4:8], mixer[8:]
     loads[3].wait()
-    put(sma, 0, dot(scaled, wq[...]))
+    put(bufs_a[0], 0, dot(scaled, wq[...]))
     loads[4].wait()
-    put(sma, key_cols, dot(scaled, wk[...]))
-    put(sma, 2 * key_cols, dot(scaled, extra_weight) + square_lanes(after_first))
-    copies_a = scatter(5, sma, rma)
+    put(bufs_a[0], key_cols, dot(scaled, wk[...]))
+    put(bufs_a[0], 2 * key_cols, dot(scaled, extra_weight) + square_lanes(after_first))
+    near_a = scatter_inner(e + 1, bufs_a)
     loads[5].wait()
-    put(smb, 0, dot(scaled, wv[...]))
-    copies_b = scatter(6, smb, rmb)
+    put(bufs_b[0], 0, dot(scaled, wv[...]))
+    near_b = scatter_inner(e + 2, bufs_b)
     loads[6].wait()
-    put(smc, 0, dot(scaled, wo[...]))
-    copies_c = scatter(7, smc, rmc)
-
-    keys_sum = collect(copies_a, sma, rma)
+    put(bufs_c[0], 0, dot(scaled, wo[...]))
+    near_c = scatter_inner(e + 3, bufs_c)
+    line_a = scatter_outer(e + 4, near_a, bufs_a)
+    line_b = scatter_outer(e + 5, near_b, bufs_b)
+    line_c = scatter_outer(e + 6, near_c, bufs_c)
+
+    keys_sum = collect(line_a, bufs_a)
     extra = keys_sum[:, 2 * key_cols :]
     scale = row_scale(extra)
     for head in range(key_heads):
@@ -292,7 +372,7 @@
     for head in range(heads):
         beta_rows[:, head, :] = jnp.broadcast_to(beta_gate[:, head : head + 1], (own_rows, size))
         dec_rows[:, head, :] = jnp.broadcast_to(decay_gate[:, head : head + 1], (own_rows, size))
-    values = silu(collect(copies_b, smb, rmb) * scale)
+    values = silu(collect(line_b, bufs_b) * scale)
     for head in range(heads):
         val_rows[:, head, :] = values[:, head * size : (head + 1) * size]
 
@@ -315,27 +395,35 @@
 
     lax.fori_loop(0, own_rows, step, 0)
 
-    out_gate = silu(collect(copies_c, smc, rmc) * scale)
+    out_gate = silu(collect(line_c, bufs_c) * scale)
     for head in range(heads):
         reading = read_rows[:, head, :]
         mean = jnp.mean(reading * reading, axis=1, keepdims=True)
         normed = reading * lax.rsqrt(mean + EPS) * head_gain_ref[...]
         cols = slice(head * size, (head + 1) * size)
         nrm[kv, :, cols] = (normed * out_gate[:, cols]).astype(BF16)
-    copies = gather(8, "kv", kv, n_kv, nrm.at[kv], nrm)
+    copies = gather(e + 7, "kv", kv, n_kv, nrm.at[kv], nrm)
     loads[7].wait()
     for copy in copies:
         copy.wait_recv()
-    branch = exchange(9, dot(flat(nrm), wout[...]), parm)
+    branch = exchange(e + 8, dot(flat(nrm), wout[...]), parm)
     after_mixer = (after_first + branch).astype(BF16).astype(F32)
 
-    final = half_ffn(
-        10, after_mixer, gain_second_ref, 8, gate2, up2, down2, (s2a, r2a, s2b, r2b), hid2, par2
-    )
-    row_id = lax.broadcasted_iota(jnp.int32, (depth, piece), 0)
-    col_id = lax.broadcasted_iota(jnp.int32, (depth, piece), 1)
-    pick = jnp.where(row_id == col_id + tp * piece, 1.0, 0.0).astype(F32).astype(BF16)
-    res_out_ref[...] = dot(final, pick).astype(BF16)
+    product = half_ffn(e + 9, after_mixer, gain_second_ref, 8, gate2, up2, down2, ffn2)
+    product = product.astype(BF16)
+    copies = []
+    for off in range(1, n_tp):
+        peer = lax.rem(tp + off, n_tp)
+        fin_send[off] = dot(product, pick(peer)).astype(BF16)
+        event = e + 9 + 5 * chunks
+        copies.append(send(event, off, fin_send.at[off], fin_recv.at[off], "tp", peer))
+    mine = pick(tp)
+    own_cols = dot(after_mixer.astype(BF16), mine)
+    branch = dot(product, mine)
+    for off in range(1, n_tp):
+        copies[off - 1].wait_recv()
+        branch = branch + fin_recv[off].astype(F32)
+    res_out_ref[...] = (own_cols + 0.5 * branch).astype(BF16)
 
     for copy in pending:
         copy.wait_send()
@@ -386,24 +474,33 @@
     key_cols = query_weight.shape[1]
     val_cols = value_weight.shape[1]
     key_heads = key_cols // size
-    hp = pad_lanes(hidden)
-
+    n_in = inner_size(n_kv)
+    n_out = n_kv // n_in
     def like(x):
         return pltpu.VMEM(x.shape, x.dtype)
 
     def slots(cols):
         return pltpu.VMEM((n_kv, own_rows, cols), BF16)
 
+    def two_stage(cols):
+        near = pltpu.VMEM((n_in, n_out, own_rows, cols), BF16)
+        line = pltpu.VMEM((n_out, own_rows, cols), BF16)
+        return [near, near, line, line]
+
     def row_buf(count):
         return pltpu.VMEM((own_rows, count, size), F32)
 
     tp_slots = pltpu.VMEM((n_tp, batch, depth), BF16)
-    ffn_bufs = [slots(hp)] * 2 + [slots(hp + LANES)] * 2 + [slots(hidden), tp_slots]
+    ffn_bufs = []
+    for i, (_, cols) in enumerate(ffn_chunks(hidden)):
+        extra = LANES if i == 0 else 0
+        ffn_bufs += two_stage(2 * pad_lanes(cols) + extra) + [slots(cols)]
     mixer_bufs = (
-        [slots(2 * key_cols + LANES)] * 2
-        + [slots(val_cols)] * 4
-        + [slots(heads * size), tp_slots]
+        two_stage(2 * key_cols + LANES) + two_stage(val_cols) + two_stage(val_cols)
     )
+    final_buf = pltpu.VMEM((n_tp, batch, piece), BF16)
+    last_bufs = [tp_slots, tp_slots, final_buf, final_buf, slots(heads * size)]
+    events = 11 + 2 * len(ffn_bufs)
     big = (
         gate_first,
         up_first,
@@ -422,8 +519,8 @@
         norm_gain_first[None, :],
         norm_gain_mixer[None, :],
         norm_gain_second[None, :],
-        beta_weight,
-        decay_weight,
+        beta_weight.T,
+        decay_weight.T,
         decay_rate[None, :],
         decay_bias[None, :],
         head_gain[None, :],
@@ -442,15 +539,16 @@
         scratch_shapes=[like(x) for x in big]
         + [like(delta_state), pltpu.VMEM((n_tp, batch, piece), BF16)]
         + ffn_bufs
+        + ffn_bufs
         + mixer_bufs
-        + ffn_bufs
+        + last_bufs
         + [row_buf(2 * key_heads), row_buf(heads), row_buf(heads), row_buf(heads), row_buf(heads)]
         + [
             pltpu.SemaphoreType.DMA((len(big),)),
             pltpu.SemaphoreType.DMA((own_rows,)),
             pltpu.SemaphoreType.DMA((own_rows,)),
-            pltpu.SemaphoreType.DMA((14, most)),
-            pltpu.SemaphoreType.DMA((14, most)),
+            pltpu.SemaphoreType.DMA((events, most)),
+            pltpu.SemaphoreType.DMA((events, most)),
         ],
         compiler_params=pltpu.CompilerParams(
             collective_id=0, has_side_effects=True, vmem_limit_bytes=60 * 1024 * 1024

time: 82.4 us -> 85.3 us (1.035)
  Pallas kernels: 72.4 us -> 78.3 us
  local copies, waits for them, and re-layouts: 8.93 us -> 6.02 us
    pallas_call x1, Pallas kernels: 72.4 us -> 78.3 us  [body(): pl.pallas_call(functools.partial(kernel, n_kv, n_tp), out_shape=(jax.Shap...]
    unnamed x4 -> x2, local copies, waits for them, and re-layouts: 8.93 us -> 6.02 us
where the time goes in v2:
time: 85.3 us; the launch traced here: 85 us
  Pallas kernels  78.3 us (92%)
  local copies, waits for them, and re-layouts  6.02 us (7%)
    pallas_call x1, Pallas kernels, body(): pl.pallas_call(functools.partial(kernel, n_kv, n_tp), out_shape=(jax.Shap...  78.3 us
    unnamed x2, local copies, waits for them, and re-layouts  6.02 us

profile of v2, /device:TPU:0, one launch (start us, length us, event | category | flops | bytes accessed | tf_op | source)
XLA Modules:
  0.0 85.0 jit_solution(4830153047489091157)
XLA Ops:
  0.6 78.3 %layer.1 = (bf16[64,64]{1,0:T(8,128)(2,1)}, f32[8,8,128,128]{3,2,1,0:T(8,128)}) custom-call(bf16[64,64]{1,0:T(8,128)(2,1)} %res_ref.1, f32[1,256]{1,0:T(1,128)} %bitcast.10, f32[1,256]{1,0:T(1,128)} %bitcast.11, f32[1,256]{1,0:T(1,128)} %bitcast.12, bf16[32,256]{1,0:T(8,128)(2,1)} %bitcast.8, bf16[32,256]{1,0:T(8,128)(2,1)} %bitcast.9, f32[1,8]{1,0:T(1,128)} %bitcast.13, ...), custom_call_target="tpu_custom_call" | custom-call | tf_op jit(solution)/shard_map/layer/pallas_call | solution.py:531
  79.0 1.3 %copy.25 = bf16[64,64]{1,0:T(8,128)(2,1)} copy(bf16[64,64]{1,0:T(8,128)(2,1)} %get-tuple-element.4) | data formatting | bytes 16384
  80.3 4.7 %copy.26 = f32[8,8,128,128]{3,2,1,0:T(8,128)} copy(f32[8,8,128,128]{3,2,1,0:T(8,128)} %get-tuple-element.5) | data formatting | bytes 8388608

commit v3 on v1

--- a/solution.py
+++ b/solution.py
@@ -23,6 +23,10 @@
 
 def dot(a, b):
     return jnp.dot(a, b, preferred_element_type=F32)
+
+
+def dot_first(a, b):
+    return lax.dot_general(a, b, (((0,), (0,)), ((), ())), preferred_element_type=F32)
 
 
 def place(rows, cols, shift):
@@ -89,7 +93,8 @@
     s2b,
     r2b,
     hid2,
-    par2,
+    fin_send,
+    fin_recv,
     qk_rows,
     val_rows,
     beta_rows,
@@ -214,7 +219,7 @@
             total = total + slots[other].astype(F32)
         return total
 
-    def half_ffn(event, residual, gain_ref, first, w_gate, w_up, w_down, bufs, hid, par):
+    def half_ffn(event, residual, gain_ref, first, w_gate, w_up, w_down, bufs, hid):
         send_a, recv_a, send_b, recv_b = bufs
         hidden_cols = w_gate.shape[1]
         up_end = pad_lanes(hidden_cols)
@@ -235,8 +240,7 @@
         loads[first + 2].wait()
         for copy in copies:
             copy.wait_recv()
-        branch = exchange(event + 3, dot(flat(hid), w_down[...]), par)
-        return (residual + 0.5 * branch).astype(BF16)
+        return dot(flat(hid), w_down[...])
 
     copies = gather(0, "tp", tp, n_tp, res_ref, res_all)
     for load in loads[7:]:
@@ -245,8 +249,8 @@
         pltpu.make_async_copy(state_hbm.at[row], state.at[row], in_sem.at[row]).start()
     decay_exp = jnp.exp(rate_ref[...])
     extra_weight = (
-        dot(beta_ref[...], place_heads(beta_ref.shape[1], tp * heads, 0, heads))
-        + dot(decay_ref[...], place_heads(beta_ref.shape[1], tp * heads, heads, heads))
+        dot_first(beta_ref[...], place_heads(beta_ref.shape[0], tp * heads, 0, heads))
+        + dot_first(decay_ref[...], place_heads(beta_ref.shape[0], tp * heads, heads, heads))
     ).astype(BF16)
     residual = dot(res_ref[...], place(piece, depth, tp * piece))
     for off in range(1, n_tp):
@@ -254,9 +258,11 @@
         source = lax.rem(tp + n_tp - off, n_tp)
         residual = residual + dot(res_all[source], place(piece, depth, source * piece))
 
-    after_first = half_ffn(
-        1, residual, gain_first_ref, 0, gate1, up1, down1, (s1a, r1a, s1b, r1b), hid1, par1
-    ).astype(F32)
+    product = half_ffn(
+        1, residual, gain_first_ref, 0, gate1, up1, down1, (s1a, r1a, s1b, r1b), hid1
+    )
+    branch = exchange(4, product, par1)
+    after_first = (residual + 0.5 * branch).astype(BF16).astype(F32)
 
     scaled = (after_first * gain_mixer_ref[...]).astype(BF16)
     loads[3].wait()
@@ -329,13 +335,21 @@
     branch = exchange(9, dot(flat(nrm), wout[...]), parm)
     after_mixer = (after_first + branch).astype(BF16).astype(F32)
 
-    final = half_ffn(
-        10, after_mixer, gain_second_ref, 8, gate2, up2, down2, (s2a, r2a, s2b, r2b), hid2, par2
-    )
-    row_id = lax.broadcasted_iota(jnp.int32, (depth, piece), 0)
-    col_id = lax.broadcasted_iota(jnp.int32, (depth, piece), 1)
-    pick = jnp.where(row_id == col_id + tp * piece, 1.0, 0.0).astype(F32).astype(BF16)
-    res_out_ref[...] = dot(final, pick).astype(BF16)
+    product = half_ffn(
+        10, after_mixer, gain_second_ref, 8, gate2, up2, down2, (s2a, r2a, s2b, r2b), hid2
+    ).astype(BF16)
+    copies = []
+    for off in range(1, n_tp):
+        peer = lax.rem(tp + off, n_tp)
+        fin_send[off] = dot(product, place_back(depth, piece, peer)).astype(BF16)
+        copies.append(send(13, off, fin_send.at[off], fin_recv.at[off], "tp", peer))
+    mine = place_back(depth, piece, tp)
+    own_cols = dot(after_mixer.astype(BF16), mine)
+    branch = dot(product, mine)
+    for off in range(1, n_tp):
+        copies[off - 1].wait_recv()
+        branch = branch + fin_recv[off].astype(F32)
+    res_out_ref[...] = (own_cols + 0.5 * branch).astype(BF16)
 
     for copy in pending:
         copy.wait_send()
@@ -345,6 +359,12 @@
         return carry
 
     lax.fori_loop(0, own_rows, drain, 0)
+
+
+def place_back(rows, cols, peer):
+    row = lax.broadcasted_iota(jnp.int32, (rows, cols), 0)
+    col = lax.broadcasted_iota(jnp.int32, (rows, cols), 1)
+    return jnp.where(row == col + peer * cols, 1.0, 0.0).astype(F32).astype(BF16)
 
 
 def place_heads(rows, first, lane_start, count):
@@ -422,8 +442,8 @@
         norm_gain_first[None, :],
         norm_gain_mixer[None, :],
         norm_gain_second[None, :],
-        beta_weight,
-        decay_weight,
+        beta_weight.T,
+        decay_weight.T,
         decay_rate[None, :],
         decay_bias[None, :],
         head_gain[None, :],
@@ -443,7 +463,8 @@
         + [like(delta_state), pltpu.VMEM((n_tp, batch, piece), BF16)]
         + ffn_bufs
         + mixer_bufs
-        + ffn_bufs
+        + ffn_bufs[:-1]
+        + [pltpu.VMEM((n_tp, batch, piece), BF16)] * 2
         + [row_buf(2 * key_heads), row_buf(heads), row_buf(heads), row_buf(heads), row_buf(heads)]
         + [
             pltpu.SemaphoreType.DMA((len(big),)),

time: 82.4 us -> 79.1 us (0.960)
  local copies, waits for them, and re-layouts: 8.93 us -> 6.02 us
    unnamed x4 -> x2, local copies, waits for them, and re-layouts: 8.93 us -> 6.02 us
where the time goes in v3:
time: 79.1 us; the launch traced here: 78.9 us
  Pallas kernels  72.2 us (91%)
  local copies, waits for them, and re-layouts  6.02 us (8%)
    pallas_call x1, Pallas kernels, body(): pl.pallas_call(functools.partial(kernel, n_kv, n_tp), out_shape=(jax.Shap...  72.2 us
    unnamed x2, local copies, waits for them, and re-layouts  6.02 us

profile of v3, /device:TPU:0, one launch (start us, length us, event | category | flops | bytes accessed | tf_op | source)
XLA Modules:
  0.0 78.9 jit_solution(5585662020206882538)
XLA Ops:
  0.6 72.2 %layer.1 = (bf16[64,64]{1,0:T(8,128)(2,1)}, f32[8,8,128,128]{3,2,1,0:T(8,128)}) custom-call(bf16[64,64]{1,0:T(8,128)(2,1)} %res_ref.1, f32[1,256]{1,0:T(1,128)} %bitcast.10, f32[1,256]{1,0:T(1,128)} %bitcast.11, f32[1,256]{1,0:T(1,128)} %bitcast.12, bf16[32,256]{1,0:T(8,128)(2,1)} %bitcast.8, bf16[32,256]{1,0:T(8,128)(2,1)} %bitcast.9, f32[1,8]{1,0:T(1,128)} %bitcast.13, ...), custom_call_target="tpu_custom_call" | custom-call | tf_op jit(solution)/shard_map/layer/pallas_call | solution.py:454
  72.8 1.3 %copy.25 = bf16[64,64]{1,0:T(8,128)(2,1)} copy(bf16[64,64]{1,0:T(8,128)(2,1)} %get-tuple-element.4) | data formatting | bytes 16384
  74.2 4.7 %copy.26 = f32[8,8,128,128]{3,2,1,0:T(8,128)} copy(f32[8,8,128,128]{3,2,1,0:T(8,128)} %get-tuple-element.5) | data formatting | bytes 8388608
